TPU v7x, 32 devices: a whole 2x2x4 slice. The times are simulated.
32 devices in a mesh: sp: 8 (over z, y), dp: 4 (over x, core).
Axes of the slice: x: 2, y: 2, z: 4, core: 2. Of those that a mesh axis runs over, the one named last changes fastest.
Arguments:
- tokens: bfloat16 [4, 512, 1024], P('dp', 'sp'), may hold values from -6 to 6
- w_query: bfloat16 [1024, 512], P(None, ('sp', 'dp')), may hold values from -0.1875 to 0.1875
- w_forward: bfloat16 [1024, 512], P(None, ('sp', 'dp')), may hold values from -0.1875 to 0.1875
- w_backward: bfloat16 [1024, 512], P(None, ('sp', 'dp')), may hold values from -0.1875 to 0.1875
- w_input: bfloat16 [1024, 512], P(None, ('sp', 'dp')), may hold values from -0.1875 to 0.1875
- w_gate: bfloat16 [1024, 512], P(None, ('sp', 'dp')), may hold values from -0.1875 to 0.1875
- w_out: bfloat16 [512, 1024], P(None, ('sp', 'dp')), may hold values from -0.25 to 0.25
- memory_forward: float32 [512], replicated, may hold values from 0.3 to 4
- memory_backward: float32 [512], replicated, may hold values from 0.3 to 4
- norm_gain: float32 [128], replicated, may hold values from 0.1 to 1.9
Outputs:
- mixed: bfloat16 [4, 512, 1024], P('dp', 'sp')
All inputs are finite; a program needn't handle non-finite values.
Results may differ from a plain program's by a relative error of at most 0.015.
Values may be sent and summed in bfloat16 or wider, within the bound.
A program may use at most 64 MiB of HBM per device.

v0:
```python
import jax
import jax.numpy as jnp
from jax import lax
from jax.sharding import PartitionSpec as P

HEADS = 4
HEAD_DIM = 128
BLOCK = 64
norm_eps = 1e-06
highest = lax.Precision.HIGHEST


def as_sent(array):
    return jax.tree.map(lambda a: a.astype(jnp.bfloat16) if a.dtype == jnp.float32 else a, array)


def gathered_then(share, axis, dim, apply):
    everything = lax.all_gather(share, axis, axis=dim, tiled=True)
    return apply(everything, jnp.int32(0))


def log_forget(projected, memory, seq_len):
    slack_value = memory / seq_len
    return jnp.logaddexp(
        jnp.log1p(-slack_value),
        jnp.log(slack_value) + jax.nn.log_sigmoid(projected.astype(jnp.float32)),
    )


def sweep(queries, log_decay, values):
    seq_len, key_width = queries.shape
    blocks = seq_len // BLOCK
    input_keys = -jnp.expm1(log_decay)
    lower_mask = jnp.tril(jnp.ones((BLOCK, BLOCK), dtype=bool))[:, :, None]

    def advance(carry_state, inputs):
        query_part, decay_part, key_part, value_part = inputs
        running = jnp.cumsum(decay_part, axis=0)
        from_state = jnp.dot(query_part * jnp.exp(running), carry_state, precision=highest)
        gaps = running[:, None, :] - running[None, :, :]
        decay_table = jnp.where(lower_mask, jnp.exp(jnp.where(lower_mask, gaps, 0.0)), 0.0)
        scores = jnp.sum(query_part[:, None, :] * key_part[None, :, :] * decay_table, axis=2)
        inside = jnp.dot(scores, value_part, precision=highest)
        final_sum = running[-1]
        weighted = key_part * jnp.exp(final_sum[None, :] - running)
        carry_state = jnp.exp(final_sum)[:, None] * carry_state + jnp.dot(
            weighted.T, value_part, precision=highest
        )
        return (carry_state, from_state + inside)

    def blocked(array):
        return array.reshape(blocks, BLOCK, array.shape[1])

    zero_state = jnp.zeros((key_width, values.shape[1]), jnp.float32)
    _, readings = lax.scan(
        advance,
        zero_state,
        (blocked(queries), blocked(log_decay), blocked(input_keys), blocked(values)),
    )
    return readings.reshape(seq_len, values.shape[1])


def both_ways(queries, log_ahead, log_behind, values):
    forward_read = sweep(queries, log_ahead, values)
    behind = sweep(jnp.flip(queries, 0), jnp.flip(log_behind, 0), jnp.flip(values, 0))
    return forward_read + jnp.flip(behind, 0)


def body(
    tokens,
    w_query,
    w_forward,
    w_backward,
    w_input,
    w_gate,
    w_out,
    memory_forward,
    memory_backward,
    norm_gain,
):
    seq_count, tok_count, model_width = tokens.shape
    row_count = seq_count * tok_count
    flat_tokens = tokens.reshape(row_count, model_width)
    group_count = lax.axis_size("sp")
    per_head_groups = group_count // HEADS
    block_width = HEAD_DIM // per_head_groups
    head_index = lax.axis_index("sp") // per_head_groups
    full_query, full_forward, full_backward, full_input, full_gate = (
        lax.all_gather(w_query, ("sp", "dp"), axis=1, tiled=True),
        lax.all_gather(w_forward, ("sp", "dp"), axis=1, tiled=True),
        lax.all_gather(w_backward, ("sp", "dp"), axis=1, tiled=True),
        lax.all_gather(w_input, ("sp", "dp"), axis=1, tiled=True),
        lax.all_gather(w_gate, ("sp", "dp"), axis=1, tiled=True),
    )

    def project(weight):
        return jnp.dot(flat_tokens, weight, preferred_element_type=jnp.float32).astype(jnp.bfloat16)

    def by_head(projected):
        shaped = projected.reshape(row_count, HEADS, 1, HEAD_DIM)
        spread_out = jnp.broadcast_to(shaped, (row_count, HEADS, per_head_groups, HEAD_DIM))
        return spread_out.reshape(row_count, group_count, HEAD_DIM)

    def by_group(projected):
        return projected.reshape(row_count, group_count, block_width)

    query_heads, ahead_heads, behind_heads, value_heads = (
        lax.all_to_all(
            as_sent(by_head(project(full_query))), "sp", split_axis=1, concat_axis=0, tiled=True
        ),
        lax.all_to_all(
            as_sent(by_head(project(full_forward))), "sp", split_axis=1, concat_axis=0, tiled=True
        ),
        lax.all_to_all(
            as_sent(by_head(project(full_backward))), "sp", split_axis=1, concat_axis=0, tiled=True
        ),
        lax.all_to_all(
            as_sent(by_group(project(full_input))), "sp", split_axis=1, concat_axis=0, tiled=True
        ),
    )
    gate_rows = project(full_gate)
    seq_len = query_heads.shape[0]
    memory_ahead = lax.dynamic_slice_in_dim(memory_forward, head_index * HEAD_DIM, HEAD_DIM)
    memory_behind = lax.dynamic_slice_in_dim(memory_backward, head_index * HEAD_DIM, HEAD_DIM)
    queries = jax.nn.silu(query_heads[:, 0].astype(jnp.float32))
    log_ahead = log_forget(ahead_heads[:, 0], memory_ahead, seq_len)
    log_behind = log_forget(behind_heads[:, 0], memory_behind, seq_len)
    values = value_heads[:, 0].astype(jnp.float32)
    readout = both_ways(queries, log_ahead, log_behind, values).astype(jnp.bfloat16)
    returned = lax.all_to_all(
        readout.reshape(seq_len, 1, block_width), "sp", split_axis=0, concat_axis=1, tiled=True
    )
    readout_rows = returned.reshape(row_count, HEADS, HEAD_DIM).astype(jnp.float32)
    normed = (
        readout_rows
        * lax.rsqrt(jnp.mean(readout_rows * readout_rows, axis=-1, keepdims=True) + norm_eps)
        * norm_gain
    )
    normed = normed.reshape(row_count, HEADS * HEAD_DIM)
    gated_rows = (normed * jax.nn.silu(gate_rows.astype(jnp.float32))).astype(jnp.bfloat16)

    def output_block(weight_piece, first_index):
        return jnp.dot(gated_rows, weight_piece, preferred_element_type=jnp.float32).astype(
            jnp.bfloat16
        )

    mixed_rows = gathered_then(w_out, ("sp", "dp"), 1, output_block)
    return mixed_rows.reshape(seq_count, tok_count, model_width)


def solution(mesh):
    return jax.shard_map(
        body,
        mesh=mesh,
        in_specs=(
            P("dp", "sp", None),
            P(None, ("sp", "dp")),
            P(None, ("sp", "dp")),
            P(None, ("sp", "dp")),
            P(None, ("sp", "dp")),
            P(None, ("sp", "dp")),
            P(None, ("sp", "dp")),
            P(),
            P(),
            P(),
        ),
        out_specs=P("dp", "sp", None),
        check_vma=False,
    )
```

profile of v0, /device:TPU:0, one launch (start us, length us, event | category | flops | bytes accessed | tf_op | source)
XLA Modules:
  0.0 354.7 jit_solution(13744162278260831660)
XLA Ops:
  6.5 0.7 all-gather.13.cloned.1.call-update
  7.3 0.7 all-gather.9.cloned.1.call-update
  8.1 0.7 all-gather.11.cloned.1.call-update
  8.8 0.5 all-gather.7.cloned.1.call-update
  9.4 0.5 all-gather.15.cloned.1.call-update
  10.0 0.5 all-gather.17.cloned.1.call-update
  10.5 0.8 negate_log-plus-one_fusion
  11.3 0.8 negate_log-plus-one_fusion.1
  12.1 54.5 %all-gather.13.cloned.1.call-done = bf16[1024,512]{0,1:T(8,128)(2,1)} async-done(((bf16[1024,16]{0,1:T(8,128)(2,1)}), bf16[1024,512]{0,1:T(8,128)(2,1)}) %all-gather.13.cloned.1.call-update) | async-done | bytes 1048592 | tf_op jit(solution)/shard_map/all_gather | solution.py:91
  66.6 1.7 fusion.54
  68.2 53.8 %all-gather.9.cloned.1.call-done = bf16[1024,512]{0,1:T(8,128)(2,1)} async-done(((bf16[1024,16]{0,1:T(8,128)(2,1)}), bf16[1024,512]{0,1:T(8,128)(2,1)}) %all-gather.9.cloned.1.call-update) | async-done | bytes 1048592 | tf_op jit(solution)/shard_map/all_gather | solution.py:92
  122.0 1.7 convolution_convert_fusion.4
  123.9 0.8 reshape.264
  124.7 4.5 %all-to-all-start.1 = ((bf16[8,2,2048]{2,1,0:T(2,128)(2,1)}), bf16[8,2,2048]{2,1,0:T(2,128)(2,1)S(1)}, u32[]{:S(2)}, u32[]{:S(2)}) async-start(bf16[8,2,2048]{2,1,0:T(2,128)(2,1)} %reshape.264), calls=%async_computation.1 | async-start | bytes 131072 | tf_op jit(solution)/shard_map/all_to_all | solution.py:117
  129.2 48.4 %all-gather.11.cloned.1.call-done = bf16[1024,512]{0,1:T(8,128)(2,1)} async-done(((bf16[1024,16]{0,1:T(8,128)(2,1)}), bf16[1024,512]{0,1:T(8,128)(2,1)}) %all-gather.11.cloned.1.call-update) | async-done | bytes 1048592 | tf_op jit(solution)/shard_map/all_gather | solution.py:89
  177.5 1.7 fusion.53
  179.2 53.6 %all-gather.7.cloned.1.call-done = bf16[1024,512]{0,1:T(8,128)(2,1)} async-done(((bf16[1024,16]{0,1:T(8,128)(2,1)}), bf16[1024,512]{0,1:T(8,128)(2,1)}) %all-gather.7.cloned.1.call-update) | async-done | bytes 1048592 | tf_op jit(solution)/shard_map/all_gather | solution.py:90
  232.9 1.7 fusion.52
  234.6 0.7 broadcast_in_dim.94
  235.2 4.5 %all-to-all-start.3 = ((bf16[64,8,128]{2,0,1:T(8,128)(2,1)}), bf16[64,8,128]{2,0,1:T(8,128)(2,1)S(1)}, u32[]{:S(2)}, u32[]{:S(2)}) async-start(bf16[64,8,128]{2,0,1:T(8,128)(2,1)} %bitcast.17), calls=%async_computation.3 | async-start | bytes 262144 | tf_op jit(solution)/shard_map/all_to_all | solution.py:114
  240.1 7.1 %all-to-all-done.3 = bf16[64,8,128]{2,0,1:T(8,128)(2,1)S(1)} async-done(((bf16[64,8,128]{2,0,1:T(8,128)(2,1)}), bf16[64,8,128]{2,0,1:T(8,128)(2,1)S(1)}, u32[]{:S(2)}, u32[]{:S(2)}) %all-to-all-start.3) | async-done | bytes 131104 | tf_op jit(solution)/shard_map/all_to_all | solution.py:114
  247.1 0.7 broadcast_in_dim.92
  247.8 3.4 all-to-all-start.2
  251.2 0.3 add_select_fusion
  251.8 6.7 %all-to-all-done.2 = bf16[64,8,128]{2,0,1:T(8,128)(2,1)S(1)} async-done(((bf16[64,8,128]{2,0,1:T(8,128)(2,1)}), bf16[64,8,128]{2,0,1:T(8,128)(2,1)S(1)}, u32[]{:S(2)}, u32[]{:S(2)}) %all-to-all-start.2) | async-done | bytes 131104 | tf_op jit(solution)/shard_map/all_to_all | solution.py:108
  258.5 0.7 broadcast_in_dim.90
  259.1 3.4 all-to-all-start
  262.8 17.5 %while.29 = (s32[]{:T(128)}, f32[128,64]{0,1:T(8,128)S(1)}, f32[8,64,64]{2,1,0:T(8,128)S(1)}, f32[8,64,128]{2,1,0:T(8,128)S(1)}, f32[8,64,128]{2,1,0:T(8,128)S(1...) while((s32[]{:T(128)}, f32[128,64]{0,1:T(8,128)S(1)}, ...), condition=%wide.region_7.8_spmd.clone.clone, body=%wide.region_4.7_spmd.clone.clone.sunk | while | flops 19451908 | bytes 799868 | solution.py:55
  262.9 1.4 multiply_reduce_fusion.6
  264.7 0.2 convolution_add_fusion.7
  265.1 1.4 multiply_reduce_fusion.6
  267.3 1.4 multiply_reduce_fusion.6
  269.5 1.4 multiply_reduce_fusion.6
  271.2 0.2 convolution_add_fusion.7
  271.6 1.4 multiply_reduce_fusion.6
  273.4 0.2 convolution_add_fusion.7
  273.8 1.4 multiply_reduce_fusion.6
  275.6 0.2 convolution_add_fusion.7
  276.0 1.4 multiply_reduce_fusion.6
  278.2 1.4 multiply_reduce_fusion.6
  280.3 0.4 exponential-minus-one_negate_fusion.1
  280.8 17.5 %while.28 = (s32[]{:T(128)}, f32[128,64]{0,1:T(8,128)S(1)}, f32[8,64,64]{2,1,0:T(8,128)S(1)}, f32[8,64,128]{2,1,0:T(8,128)S(1)}, f32[8,64,128]{2,1,0:T(8,128)S(1...) while((s32[]{:T(128)}, f32[128,64]{0,1:T(8,128)S(1)}, ...), condition=%wide.region_3.4_spmd.clone.clone, body=%wide.region_0.3_spmd.clone.clone.sunk | while | flops 19451908 | bytes 799868 | solution.py:55
  280.9 1.4 multiply_reduce_fusion.5
  282.7 0.2 convolution_add_fusion.6
  283.1 1.4 multiply_reduce_fusion.5
  284.9 0.2 convolution_add_fusion.6
  285.3 1.4 multiply_reduce_fusion.5
  287.1 0.2 convolution_add_fusion.6
  287.5 1.4 multiply_reduce_fusion.5
  289.2 0.2 convolution_add_fusion.6
  289.7 1.4 multiply_reduce_fusion.5
  291.8 1.4 multiply_reduce_fusion.5
  294.0 1.4 multiply_reduce_fusion.5
  295.8 0.2 convolution_add_fusion.6
  296.2 1.4 multiply_reduce_fusion.5
  298.0 0.2 convolution_add_fusion.6
  298.4 0.3 rev.17
  298.9 0.5 broadcast.161
  299.4 0.7 reduce.4
  300.2 0.8 reshape.266
  301.0 5.9 %all-to-all-start.4 = ((bf16[8,2,2048]{2,1,0:T(2,128)(2,1)}), bf16[8,2,2048]{2,1,0:T(2,128)(2,1)S(1)}, u32[]{:S(2)}, u32[]{:S(2)}) async-start(bf16[8,2,2048]{2,1,0:T(2,128)(2,1)} %reshape.266), calls=%async_computation.4 | async-start | bytes 131072 | tf_op jit(solution)/shard_map/all_to_all | solution.py:130
  306.9 6.9 %all-to-all-done.4 = bf16[8,2,2048]{2,1,0:T(2,128)(2,1)S(1)} async-done(((bf16[8,2,2048]{2,1,0:T(2,128)(2,1)}), bf16[8,2,2048]{2,1,0:T(2,128)(2,1)S(1)}, u32[]{:S(2)}, u32[]{:S(2)}) %all-to-all-start.4) | async-done | bytes 65568 | tf_op jit(solution)/shard_map/all_to_all | solution.py:130
  314.7 29.9 %all-gather.17.cloned.1.call-done = bf16[512,1024]{0,1:T(8,128)(2,1)} async-done(((bf16[512,32]{0,1:T(8,128)(2,1)}), bf16[512,1024]{0,1:T(8,128)(2,1)}) %all-gather.17.cloned.1.call-update) | async-done | bytes 1048592 | tf_op jit(solution)/shard_map/all_gather | solution.py:18
  344.8 3.0 fusion.50
  (181 shorter events, 11.9 us)
Async XLA Ops:
  6.5 60.0 %copy-start = (bf16[1,64,1024]{2,1,0:T(8,128)(2,1)S(1)}, bf16[1,64,1024]{2,1,0:T(8,128)(2,1)}, u32[]{:S(2)}) copy-start(bf16[1,64,1024]{2,1,0:T(8,128)(2,1)} %param.14) | copy-start | bytes 393220
  6.5 60.0 %all-gather.13.cloned.1.call-start = ((), (), s32[]{:S(2)}) async-start(), calls=%async_computation.8 | async-start | bytes 1081344 | tf_op jit(solution)/shard_map/all_gather | solution.py:91
  7.3 114.8 %all-gather.9.cloned.1.call-start = ((), (), s32[]{:S(2)}) async-start(), calls=%async_computation.6 | async-start | bytes 1081344 | tf_op jit(solution)/shard_map/all_gather | solution.py:92
  8.0 169.5 %all-gather.11.cloned.1.call-start = ((), (), s32[]{:S(2)}) async-start(), calls=%async_computation.7 | async-start | bytes 1081344 | tf_op jit(solution)/shard_map/all_gather | solution.py:89
  8.7 224.1 %all-gather.7.cloned.1.call-start = ((), (), s32[]{:S(2)}) async-start(), calls=%async_computation.5 | async-start | bytes 1081344 | tf_op jit(solution)/shard_map/all_gather | solution.py:90
  9.3 305.4 %all-gather.15.cloned.1.call-start = ((), (), s32[]{:S(2)}) async-start(), calls=%async_computation.9 | async-start | bytes 1081344 | tf_op jit(solution)/shard_map/all_gather | solution.py:93
  9.9 334.8 %all-gather.17.cloned.1.call-start = ((), (), s32[]{:S(2)}) async-start(), calls=%async_computation.10 | async-start | bytes 1081344 | tf_op jit(solution)/shard_map/all_gather | solution.py:18
  124.7 109.9 %all-to-all-start.1 = ((bf16[8,2,2048]{2,1,0:T(2,128)(2,1)}), bf16[8,2,2048]{2,1,0:T(2,128)(2,1)S(1)}, u32[]{:S(2)}, u32[]{:S(2)}) async-start(bf16[8,2,2048]{2,1,0:T(2,128)(2,1)} %reshape.264), calls=%async_computation.1 | async-start | bytes 131072 | tf_op jit(solution)/shard_map/all_to_all | solution.py:117
  235.2 11.9 %all-to-all-start.3 = ((bf16[64,8,128]{2,0,1:T(8,128)(2,1)}), bf16[64,8,128]{2,0,1:T(8,128)(2,1)S(1)}, u32[]{:S(2)}, u32[]{:S(2)}) async-start(bf16[64,8,128]{2,0,1:T(8,128)(2,1)} %bitcast.17), calls=%async_computation.3 | async-start | bytes 262144 | tf_op jit(solution)/shard_map/all_to_all | solution.py:114
  247.8 10.7 %all-to-all-start.2 = ((bf16[64,8,128]{2,0,1:T(8,128)(2,1)}), bf16[64,8,128]{2,0,1:T(8,128)(2,1)S(1)}, u32[]{:S(2)}, u32[]{:S(2)}) async-start(bf16[64,8,128]{2,0,1:T(8,128)(2,1)} %bitcast.10), calls=%async_computation.2 | async-start | bytes 262144 | tf_op jit(solution)/shard_map/all_to_all | solution.py:108
  259.1 21.2 %all-to-all-start = ((bf16[64,8,128]{2,0,1:T(8,128)(2,1)}), bf16[64,8,128]{2,0,1:T(8,128)(2,1)S(1)}, u32[]{:S(2)}, u32[]{:S(2)}) async-start(bf16[64,8,128]{2,0,1:T(8,128)(2,1)} %bitcast.1), calls=%async_computation | async-start | bytes 262144 | tf_op jit(solution)/shard_map/all_to_all | solution.py:111
  298.2 8.7 %copy-start.1 = (f32[128]{0:T(128)S(1)}, f32[128]{0:T(128)}, u32[]{:S(2)}) copy-start(f32[128]{0:T(128)} %param.23) | copy-start | bytes 1540
  301.0 12.8 %all-to-all-start.4 = ((bf16[8,2,2048]{2,1,0:T(2,128)(2,1)}), bf16[8,2,2048]{2,1,0:T(2,128)(2,1)S(1)}, u32[]{:S(2)}, u32[]{:S(2)}) async-start(bf16[8,2,2048]{2,1,0:T(2,128)(2,1)} %reshape.266), calls=%async_computation.4 | async-start | bytes 131072 | tf_op jit(solution)/shard_map/all_to_all | solution.py:130
Sparse Core Ops, SparseCore 0:
  10.2 56.3 all-gather.12
  69.4 52.5 all-gather.8
  124.9 52.5 all-gather.10
  180.2 52.5 all-gather.6
  235.6 53.3 all-gather.14
  291.7 52.8 all-gather.16
where the time goes:
time: 355 us
  waiting for transfers between devices  265 us (75%)
  other arithmetic  26.9 us (8%)
  starting transfers between devices  21.8 us (6%)
  matrix products  19.3 us (5%)
  between operations  13.8 us (4%)
  local copies, waits for them, and re-layouts  6.91 us (2%)
    all_gather x1, waiting for transfers between devices, body(): lax.all_gather(w_backward, ('sp', 'dp'), axis=1, tiled=True)  54.5 us
    all_gather x1, waiting for transfers between devices, body(): lax.all_gather(w_input, ('sp', 'dp'), axis=1, tiled=True)  53.8 us
    all_gather x1, waiting for transfers between devices, body(): lax.all_gather(w_forward, ('sp', 'dp'), axis=1, tiled=True)  53.6 us
    all_gather x1, waiting for transfers between devices, body(): lax.all_gather(w_query, ('sp', 'dp'), axis=1, tiled=True)  48.4 us
    all_gather x1, waiting for transfers between devices, gathered_then(): everything = lax.all_gather(share, axis, axis=dim, tiled=True)  29.9 us
    reduce_sum x16, other arithmetic, advance(): jnp.sum(query_part[:, None, :] * key_part[None, :, :] * decay_table, axis=2)  21.8 us
  transfers between devices with their start and end apart: 11, of which 8 were waited for; matrix products, arithmetic and copies ran while one was open for 14% of the time, Pallas kernels for 0%

commit v1 on v0

--- a/solution.py
+++ b/solution.py
@@ -86,7 +86,7 @@
     block_width = HEAD_DIM // per_head_groups
     head_index = lax.axis_index("sp") // per_head_groups
     full_query, full_forward, full_backward, full_input, full_gate = (
-        lax.all_gather(w_query, ("sp", "dp"), axis=1, tiled=True),
+        jnp.concatenate(lax.all_gather(w_query, ("sp", "dp")), axis=1),
         lax.all_gather(w_forward, ("sp", "dp"), axis=1, tiled=True),
         lax.all_gather(w_backward, ("sp", "dp"), axis=1, tiled=True),
         lax.all_gather(w_input, ("sp", "dp"), axis=1, tiled=True),

time: 355 us -> 355 us (level)
    all_gather x1, waiting for transfers between devices: 53.6 us -> 48.2 us  [body(): lax.all_gather(w_forward, ('sp', 'dp'), axis=1, tiled=True)]
    all_gather x1, waiting for transfers between devices: 48.4 us -> 53.8 us  [body(): lax.all_gather(w_query, ('sp', 'dp'))]
where the time goes in v1:
time: 355 us
  waiting for transfers between devices  263 us (74%)
  other arithmetic  26.9 us (8%)
  starting transfers between devices  21.9 us (6%)
  matrix products  18.1 us (5%)
  between operations  13.8 us (4%)
  local copies, waits for them, and re-layouts  9.3 us (3%)
    all_gather x1, waiting for transfers between devices, body(): lax.all_gather(w_backward, ('sp', 'dp'), axis=1, tiled=True)  54.5 us
    all_gather x1, waiting for transfers between devices, body(): lax.all_gather(w_query, ('sp', 'dp'))  53.8 us
    all_gather x1, waiting for transfers between devices, body(): lax.all_gather(w_input, ('sp', 'dp'), axis=1, tiled=True)  52.7 us
    all_gather x1, waiting for transfers between devices, body(): lax.all_gather(w_forward, ('sp', 'dp'), axis=1, tiled=True)  48.2 us
    all_gather x1, waiting for transfers between devices, gathered_then(): everything = lax.all_gather(share, axis, axis=dim, tiled=True)  29.9 us
    reduce_sum x16, other arithmetic, advance(): jnp.sum(query_part[:, None, :] * key_part[None, :, :] * decay_table, axis=2)  21.8 us
  transfers between devices with their start and end apart: 11, of which 8 were waited for; matrix products, arithmetic and copies ran while one was open for 14% of the time, Pallas kernels for 0%

profile of v1, /device:TPU:0, one launch (start us, length us, event | category | flops | bytes accessed | tf_op | source)
XLA Modules:
  0.0 354.7 jit_solution(8051969633142091391)
XLA Ops:
  6.5 0.7 all-gather.12.cloned.1.call-update
  7.3 0.7 all-gather.18.cloned.1.call-update
  8.1 0.7 all-gather.10.cloned.1.call-update
  8.8 0.5 all-gather.8.cloned.1.call-update
  9.4 0.5 all-gather.14.cloned.1.call-update
  10.0 0.5 all-gather.16.cloned.1.call-update
  10.5 0.8 negate_log-plus-one_fusion
  11.3 0.8 negate_log-plus-one_fusion.1
  12.1 54.5 %all-gather.12.cloned.1.call-done = bf16[1024,512]{0,1:T(8,128)(2,1)} async-done(((bf16[1024,16]{0,1:T(8,128)(2,1)}), bf16[1024,512]{0,1:T(8,128)(2,1)}) %all-gather.12.cloned.1.call-update) | async-done | bytes 1048592 | tf_op jit(solution)/shard_map/all_gather | solution.py:91
  66.6 1.7 fusion.54
  68.2 53.8 %all-gather.18.cloned.1.call-done = bf16[32768,16]{0,1:T(8,128)(2,1)} async-done(((bf16[1024,16]{0,1:T(8,128)(2,1)}), bf16[32768,16]{0,1:T(8,128)(2,1)}) %all-gather.18.cloned.1.call-update) | async-done | bytes 1048592 | tf_op jit(solution)/shard_map/all_gather | solution.py:89
  122.0 1.8 copy.88
  123.8 0.6 copy.72
  124.4 0.4 fusion.53
  124.9 52.7 %all-gather.10.cloned.1.call-done = bf16[1024,512]{0,1:T(8,128)(2,1)} async-done(((bf16[1024,16]{0,1:T(8,128)(2,1)}), bf16[1024,512]{0,1:T(8,128)(2,1)}) %all-gather.10.cloned.1.call-update) | async-done | bytes 1048592 | tf_op jit(solution)/shard_map/all_gather | solution.py:92
  177.5 1.7 convolution_convert_fusion.4
  179.4 0.8 reshape.273
  180.2 4.5 %all-to-all-start.1 = ((bf16[8,2,2048]{2,1,0:T(2,128)(2,1)}), bf16[8,2,2048]{2,1,0:T(2,128)(2,1)S(1)}, u32[]{:S(2)}, u32[]{:S(2)}) async-start(bf16[8,2,2048]{2,1,0:T(2,128)(2,1)} %reshape.273), calls=%async_computation.1 | async-start | bytes 131072 | tf_op jit(solution)/shard_map/all_to_all | solution.py:117
  184.7 48.2 %all-gather.8.cloned.1.call-done = bf16[1024,512]{0,1:T(8,128)(2,1)} async-done(((bf16[1024,16]{0,1:T(8,128)(2,1)}), bf16[1024,512]{0,1:T(8,128)(2,1)}) %all-gather.8.cloned.1.call-update) | async-done | bytes 1048592 | tf_op jit(solution)/shard_map/all_gather | solution.py:90
  232.9 1.7 fusion.52
  234.6 0.7 broadcast_in_dim.94
  235.2 4.5 %all-to-all-start.3 = ((bf16[64,8,128]{2,0,1:T(8,128)(2,1)}), bf16[64,8,128]{2,0,1:T(8,128)(2,1)S(1)}, u32[]{:S(2)}, u32[]{:S(2)}) async-start(bf16[64,8,128]{2,0,1:T(8,128)(2,1)} %bitcast.19), calls=%async_computation.3 | async-start | bytes 262144 | tf_op jit(solution)/shard_map/all_to_all | solution.py:114
  240.1 7.1 %all-to-all-done.3 = bf16[64,8,128]{2,0,1:T(8,128)(2,1)S(1)} async-done(((bf16[64,8,128]{2,0,1:T(8,128)(2,1)}), bf16[64,8,128]{2,0,1:T(8,128)(2,1)S(1)}, u32[]{:S(2)}, u32[]{:S(2)}) %all-to-all-start.3) | async-done | bytes 131104 | tf_op jit(solution)/shard_map/all_to_all | solution.py:114
  247.1 0.7 broadcast_in_dim.92
  247.8 3.4 all-to-all-start.2
  251.2 0.3 add_select_fusion
  251.8 6.7 %all-to-all-done.2 = bf16[64,8,128]{2,0,1:T(8,128)(2,1)S(1)} async-done(((bf16[64,8,128]{2,0,1:T(8,128)(2,1)}), bf16[64,8,128]{2,0,1:T(8,128)(2,1)S(1)}, u32[]{:S(2)}, u32[]{:S(2)}) %all-to-all-start.2) | async-done | bytes 131104 | tf_op jit(solution)/shard_map/all_to_all | solution.py:108
  258.5 0.7 broadcast_in_dim.90
  259.1 3.4 all-to-all-start
  262.8 17.5 %while.29 = (s32[]{:T(128)}, f32[128,64]{0,1:T(8,128)S(1)}, f32[8,64,64]{2,1,0:T(8,128)S(1)}, f32[8,64,128]{2,1,0:T(8,128)S(1)}, f32[8,64,128]{2,1,0:T(8,128)S(1...) while((s32[]{:T(128)}, f32[128,64]{0,1:T(8,128)S(1)}, ...), condition=%wide.region_7.8_spmd.clone.clone, body=%wide.region_4.7_spmd.clone.clone.sunk | while | flops 19451908 | bytes 799868 | solution.py:55
  262.9 1.4 multiply_reduce_fusion.6
  265.1 1.4 multiply_reduce_fusion.6
  266.9 0.2 convolution_add_fusion.7
  267.3 1.4 multiply_reduce_fusion.6
  269.1 0.2 convolution_add_fusion.7
  269.5 1.4 multiply_reduce_fusion.6
  271.2 0.2 convolution_add_fusion.7
  271.7 1.4 multiply_reduce_fusion.6
  273.8 1.4 multiply_reduce_fusion.6
  276.0 1.4 multiply_reduce_fusion.6
  277.8 0.2 convolution_add_fusion.7
  278.2 1.4 multiply_reduce_fusion.6
  280.0 0.2 convolution_add_fusion.7
  280.3 0.4 exponential-minus-one_negate_fusion.1
  280.8 17.5 %while.28 = (s32[]{:T(128)}, f32[128,64]{0,1:T(8,128)S(1)}, f32[8,64,64]{2,1,0:T(8,128)S(1)}, f32[8,64,128]{2,1,0:T(8,128)S(1)}, f32[8,64,128]{2,1,0:T(8,128)S(1...) while((s32[]{:T(128)}, f32[128,64]{0,1:T(8,128)S(1)}, ...), condition=%wide.region_3.4_spmd.clone.clone, body=%wide.region_0.3_spmd.clone.clone.sunk | while | flops 19451908 | bytes 799868 | solution.py:55
  280.9 1.4 multiply_reduce_fusion.5
  282.7 0.2 convolution_add_fusion.6
  283.1 1.4 multiply_reduce_fusion.5
  285.3 1.4 multiply_reduce_fusion.5
  287.5 1.4 multiply_reduce_fusion.5
  289.7 1.4 multiply_reduce_fusion.5
  291.4 0.2 convolution_add_fusion.6
  291.9 1.4 multiply_reduce_fusion.5
  294.0 1.4 multiply_reduce_fusion.5
  295.8 0.2 convolution_add_fusion.6
  296.2 1.4 multiply_reduce_fusion.5
  298.4 0.3 rev.17
  298.9 0.5 broadcast.161
  299.4 0.7 reduce.4
  300.2 0.8 reshape.275
  301.0 5.9 %all-to-all-start.4 = ((bf16[8,2,2048]{2,1,0:T(2,128)(2,1)}), bf16[8,2,2048]{2,1,0:T(2,128)(2,1)S(1)}, u32[]{:S(2)}, u32[]{:S(2)}) async-start(bf16[8,2,2048]{2,1,0:T(2,128)(2,1)} %reshape.275), calls=%async_computation.4 | async-start | bytes 131072 | tf_op jit(solution)/shard_map/all_to_all | solution.py:130
  306.9 6.9 %all-to-all-done.4 = bf16[8,2,2048]{2,1,0:T(2,128)(2,1)S(1)} async-done(((bf16[8,2,2048]{2,1,0:T(2,128)(2,1)}), bf16[8,2,2048]{2,1,0:T(2,128)(2,1)S(1)}, u32[]{:S(2)}, u32[]{:S(2)}) %all-to-all-start.4) | async-done | bytes 65568 | tf_op jit(solution)/shard_map/all_to_all | solution.py:130
  314.8 29.9 %all-gather.16.cloned.1.call-done = bf16[512,1024]{0,1:T(8,128)(2,1)} async-done(((bf16[512,32]{0,1:T(8,128)(2,1)}), bf16[512,1024]{0,1:T(8,128)(2,1)}) %all-gather.16.cloned.1.call-update) | async-done | bytes 1048592 | tf_op jit(solution)/shard_map/all_gather | solution.py:18
  344.8 3.0 fusion.50
  (183 shorter events, 12.4 us)
Async XLA Ops:
  6.5 60.0 %copy-start = (bf16[1,64,1024]{2,1,0:T(8,128)(2,1)S(1)}, bf16[1,64,1024]{2,1,0:T(8,128)(2,1)}, u32[]{:S(2)}) copy-start(bf16[1,64,1024]{2,1,0:T(8,128)(2,1)} %param.14) | copy-start | bytes 393220
  6.5 60.0 %all-gather.12.cloned.1.call-start = ((), (), s32[]{:S(2)}) async-start(), calls=%async_computation.7 | async-start | bytes 1081344 | tf_op jit(solution)/shard_map/all_gather | solution.py:91
  7.3 114.8 %all-gather.18.cloned.1.call-start = ((), (), s32[]{:S(2)}) async-start(), calls=%async_computation.10 | async-start | bytes 1081344 | tf_op jit(solution)/shard_map/all_gather | solution.py:89
  8.0 169.5 %all-gather.10.cloned.1.call-start = ((), (), s32[]{:S(2)}) async-start(), calls=%async_computation.6 | async-start | bytes 1081344 | tf_op jit(solution)/shard_map/all_gather | solution.py:92
  8.7 224.1 %all-gather.8.cloned.1.call-start = ((), (), s32[]{:S(2)}) async-start(), calls=%async_computation.5 | async-start | bytes 1081344 | tf_op jit(solution)/shard_map/all_gather | solution.py:90
  9.3 305.4 %all-gather.14.cloned.1.call-start = ((), (), s32[]{:S(2)}) async-start(), calls=%async_computation.8 | async-start | bytes 1081344 | tf_op jit(solution)/shard_map/all_gather | solution.py:93
  9.9 334.8 %all-gather.16.cloned.1.call-start = ((), (), s32[]{:S(2)}) async-start(), calls=%async_computation.9 | async-start | bytes 1081344 | tf_op jit(solution)/shard_map/all_gather | solution.py:18
  180.2 54.4 %all-to-all-start.1 = ((bf16[8,2,2048]{2,1,0:T(2,128)(2,1)}), bf16[8,2,2048]{2,1,0:T(2,128)(2,1)S(1)}, u32[]{:S(2)}, u32[]{:S(2)}) async-start(bf16[8,2,2048]{2,1,0:T(2,128)(2,1)} %reshape.273), calls=%async_computation.1 | async-start | bytes 131072 | tf_op jit(solution)/shard_map/all_to_all | solution.py:117
  235.2 11.9 %all-to-all-start.3 = ((bf16[64,8,128]{2,0,1:T(8,128)(2,1)}), bf16[64,8,128]{2,0,1:T(8,128)(2,1)S(1)}, u32[]{:S(2)}, u32[]{:S(2)}) async-start(bf16[64,8,128]{2,0,1:T(8,128)(2,1)} %bitcast.19), calls=%async_computation.3 | async-start | bytes 262144 | tf_op jit(solution)/shard_map/all_to_all | solution.py:114
  247.8 10.7 %all-to-all-start.2 = ((bf16[64,8,128]{2,0,1:T(8,128)(2,1)}), bf16[64,8,128]{2,0,1:T(8,128)(2,1)S(1)}, u32[]{:S(2)}, u32[]{:S(2)}) async-start(bf16[64,8,128]{2,0,1:T(8,128)(2,1)} %bitcast.12), calls=%async_computation.2 | async-start | bytes 262144 | tf_op jit(solution)/shard_map/all_to_all | solution.py:108
  259.1 21.2 %all-to-all-start = ((bf16[64,8,128]{2,0,1:T(8,128)(2,1)}), bf16[64,8,128]{2,0,1:T(8,128)(2,1)S(1)}, u32[]{:S(2)}, u32[]{:S(2)}) async-start(bf16[64,8,128]{2,0,1:T(8,128)(2,1)} %bitcast.1), calls=%async_computation | async-start | bytes 262144 | tf_op jit(solution)/shard_map/all_to_all | solution.py:111
  298.3 8.7 %copy-start.1 = (f32[128]{0:T(128)S(1)}, f32[128]{0:T(128)}, u32[]{:S(2)}) copy-start(f32[128]{0:T(128)} %param.23) | copy-start | bytes 1540
  301.0 12.8 %all-to-all-start.4 = ((bf16[8,2,2048]{2,1,0:T(2,128)(2,1)}), bf16[8,2,2048]{2,1,0:T(2,128)(2,1)S(1)}, u32[]{:S(2)}, u32[]{:S(2)}) async-start(bf16[8,2,2048]{2,1,0:T(2,128)(2,1)} %reshape.275), calls=%async_computation.4 | async-start | bytes 131072 | tf_op jit(solution)/shard_map/all_to_all | solution.py:130
Sparse Core Ops, SparseCore 0:
  10.2 56.3 all-gather.11
  69.5 52.5 all-gather.17
  124.9 52.5 all-gather.9
  180.3 52.5 all-gather.7
  235.6 53.3 all-gather.13
  291.7 52.8 all-gather.15
